TPU v7x, 32 devices: a whole 2x2x4 slice. The times are simulated.
32 devices in a mesh: ep: 8 (over z, x), tp: 4 (over y, core).
Axes of the slice: x: 2, y: 2, z: 4, core: 2. Of those that a mesh axis runs over, the one named last changes fastest.
Arguments:
- tokens: bfloat16 [1024, 2048], P('ep'), may hold values from -16 to 16
- routes: int32 [1024, 2], P('ep'), may hold values from 0 to 7, all different within a row; in each aligned block of 128 rows (0 to 127, 128 to 255, ...) at most 48 rows name the same one
- router: bfloat16 [2048, 8], replicated, may hold values from -0.125 to 0.125
- w_gate: bfloat16 [8, 2048, 2048], P('ep', None, 'tp'), may hold values from -0.125 to 0.125
- w_up: bfloat16 [8, 2048, 2048], P('ep', None, 'tp'), may hold values from -0.125 to 0.125
- w_down: bfloat16 [8, 2048, 2048], P('ep', 'tp'), may hold values from -0.125 to 0.125
- cotangent: bfloat16 [1024, 2048], P('ep'), may hold values from -6 to 6
Outputs:
- grad_tokens: bfloat16 [1024, 2048], P('ep', 'tp')
- grad_router: float32 [2048, 8], P('tp')
- grad_gate: float32 [8, 2048, 2048], P('ep', None, 'tp')
- grad_up: float32 [8, 2048, 2048], P('ep', None, 'tp')
- grad_down: float32 [8, 2048, 2048], P('ep', 'tp')
Inputs may be any that keep to these rules, and one draw needn't show every extreme that they name: In each aligned block of 128 rows, no expert is named by more than 48 of the block's routes, a bound that some block reaches; a row names 2 different experts.
All inputs are finite; a program needn't handle non-finite values.
Results may differ from a plain program's by a relative error of at most 0.017.
Values may be sent and summed in bfloat16 or wider, within the bound.
No kernel may reach another device: no remote copies, remote signals or barrier semaphores. Data moves between devices by JAX's collectives and lax.ppermute only.
A program may use at most 128 MiB of HBM per device.

v0:
```python
import jax
import jax.numpy as jnp
from jax import lax
from jax.sharding import PartitionSpec as P

clamp_limit = 7.0
sig_slope = 1.702


def on_device(tokens, routes, router, w_gate, w_up, w_down, cotangent):
    highest = lax.Precision.HIGHEST
    ep_count = lax.axis_size("ep")
    tp_count = lax.axis_size("tp")
    tp_index = lax.axis_index("tp")
    tok_rows = tokens.shape[0]
    model_width = tokens.shape[1]
    top_count = routes.shape[1]
    local_experts = w_gate.shape[0]
    all_experts = ep_count * local_experts
    capacity = 3 * tok_rows * top_count // (2 * all_experts)
    slot_count = all_experts * capacity
    feature_part = model_width // tp_count
    feature_start = tp_index * feature_part
    buffer_shape = (ep_count, local_experts, capacity)
    logits = jnp.dot(tokens, router, preferred_element_type=jnp.float32)
    expert_hot = routes[:, :, None] == jnp.arange(all_experts, dtype=jnp.int32)[None, None, :]
    chosen = jnp.sum(jnp.where(expert_hot, logits[:, None, :], 0.0), axis=2)
    weights = 1.0 / jnp.sum(jnp.exp(chosen[:, None, :] - chosen[:, :, None]), axis=2)
    flat_hot = expert_hot.reshape(tok_rows * top_count, all_experts).astype(jnp.int32)
    earlier = jnp.cumsum(flat_hot, axis=0) - flat_hot
    position = jnp.sum(earlier * flat_hot, axis=1).reshape(tok_rows, top_count)
    slot_of = routes * capacity + position
    select = slot_of[None, :, :] == jnp.arange(slot_count, dtype=jnp.int32)[:, None, None]
    dispatch = jnp.any(select, axis=2)
    dispatch_half = dispatch.astype(jnp.bfloat16)
    slot_weight = jnp.sum(jnp.where(select, weights[None, :, :], 0.0), axis=(1, 2))
    token_cols = lax.dynamic_slice_in_dim(tokens, feature_start, feature_part, 1)
    cot_cols = lax.dynamic_slice_in_dim(cotangent, feature_start, feature_part, 1)
    token_slots = jnp.dot(dispatch_half, token_cols, preferred_element_type=jnp.float32).astype(
        jnp.bfloat16
    )
    cot_slots = jnp.dot(dispatch_half, cot_cols, preferred_element_type=jnp.float32).astype(
        jnp.bfloat16
    )
    scaled = (slot_weight[:, None] * cot_slots).astype(jnp.bfloat16)
    sent_tok, sent_cot = (
        lax.all_to_all(
            token_slots.reshape(buffer_shape + (feature_part,)),
            "ep",
            split_axis=0,
            concat_axis=0,
            tiled=True,
        ),
        lax.all_to_all(
            scaled.reshape(buffer_shape + (feature_part,)),
            "ep",
            split_axis=0,
            concat_axis=0,
            tiled=True,
        ),
    )
    arrived, arrived_cot = (
        lax.all_gather(sent_tok, "tp", axis=3, tiled=True),
        lax.all_gather(sent_cot, "tp", axis=3, tiled=True),
    )
    pre_gate = jnp.einsum("slcd,ldf->slcf", arrived, w_gate, preferred_element_type=jnp.float32)
    pre_up = jnp.einsum("slcd,ldf->slcf", arrived, w_up, preferred_element_type=jnp.float32)
    gate_clamped = jnp.minimum(pre_gate, clamp_limit)
    up_clamped = jnp.clip(pre_up, -clamp_limit, clamp_limit)
    sigmoid_gate = jax.nn.sigmoid(sig_slope * gate_clamped)
    gated_act = gate_clamped * sigmoid_gate
    activation = ((up_clamped + 1.0) * gated_act).astype(jnp.bfloat16)
    back_act = jnp.einsum("slcd,lfd->slcf", arrived_cot, w_down, preferred_element_type=jnp.float32)
    share_part = jnp.sum(activation.astype(jnp.float32) * back_act, axis=3)
    slope_term = sigmoid_gate + sig_slope * gated_act * (1.0 - sigmoid_gate)
    d_gate = jnp.where(
        pre_gate < clamp_limit, back_act * (up_clamped + 1.0) * slope_term, 0.0
    ).astype(jnp.bfloat16)
    d_up = jnp.where(jnp.abs(pre_up) < clamp_limit, back_act * gated_act, 0.0).astype(jnp.bfloat16)
    grad_gate = jnp.einsum("slcd,slcf->ldf", arrived, d_gate, preferred_element_type=jnp.float32)
    grad_up = jnp.einsum("slcd,slcf->ldf", arrived, d_up, preferred_element_type=jnp.float32)
    grad_down = jnp.einsum(
        "slcf,slcd->lfd", activation, arrived_cot, preferred_element_type=jnp.float32
    )
    row_term = jnp.einsum("ldf,slcf->dslc", w_gate, d_gate, preferred_element_type=jnp.float32)
    input_part = lax.psum_scatter(
        (
            row_term + jnp.einsum("ldf,slcf->dslc", w_up, d_up, preferred_element_type=jnp.float32)
        ).astype(jnp.bfloat16),
        "tp",
        scatter_dimension=0,
        tiled=True,
    ).astype(jnp.float32)
    share_sum = lax.psum(share_part, "tp")
    back_input, back_share = (
        lax.all_to_all(
            input_part.astype(jnp.bfloat16), "ep", split_axis=1, concat_axis=1, tiled=True
        ).astype(input_part.dtype),
        lax.all_to_all(
            share_sum[None].astype(jnp.bfloat16), "ep", split_axis=1, concat_axis=1, tiled=True
        ).astype(jnp.float32),
    )
    back_input = back_input.reshape(feature_part, slot_count)
    back_share = back_share.reshape(slot_count)
    dispatch_full = dispatch.astype(jnp.float32)
    from_experts = lax.dot_general(
        dispatch_full, back_input, (((0,), (1,)), ((), ())), precision=highest
    )
    shares = jnp.sum(jnp.where(select, back_share[:, None, None], 0.0), axis=0)
    mixed_grad = shares - weights * jnp.sum(shares, axis=1, keepdims=True)
    d_logits = jnp.sum(jnp.where(expert_hot, mixed_grad[:, :, None], 0.0), axis=1)
    router_rows = lax.dynamic_slice_in_dim(router, feature_start, feature_part, 0).astype(
        jnp.float32
    )
    from_router = lax.dot_general(
        d_logits, router_rows, (((1,), (1,)), ((), ())), precision=highest
    )
    grad_tokens = (from_experts + from_router).astype(jnp.bfloat16)
    router_part = lax.dot_general(
        token_cols.astype(jnp.float32), d_logits, (((0,), (0,)), ((), ())), precision=highest
    )
    grad_router = lax.psum(router_part, "ep")
    return (grad_tokens, grad_router, grad_gate, grad_up, grad_down)


def solution(mesh):
    return jax.shard_map(
        on_device,
        mesh=mesh,
        in_specs=(
            P("ep", None),
            P("ep", None),
            P(),
            P("ep", None, "tp"),
            P("ep", None, "tp"),
            P("ep", "tp", None),
            P("ep", None),
        ),
        out_specs=(
            P("ep", "tp"),
            P("tp", None),
            P("ep", None, "tp"),
            P("ep", None, "tp"),
            P("ep", "tp", None),
        ),
        check_vma=False,
    )
```

profile of v0, /device:TPU:0, one launch (start us, length us, event | category | flops | bytes accessed | tf_op | source)
XLA Modules:
  0.0 159.0 jit_solution(8178199809806928618)
XLA Ops:
  7.2 0.0 copy-start
  7.2 0.0 copy-start.4
  7.2 0.0 copy-start.2
  7.2 0.0 all-gather.3.cloned.1.call-start
  7.3 0.9 copy.55
  8.2 0.1 eq.49
  8.3 0.1 eq.45
  8.5 0.6 reduce-window.6
  9.1 0.2 slice_reduce_fusion
  9.3 0.1 fusion.44
  9.4 0.1 reshape.140
  9.6 0.1 copy.57
  9.6 0.7 multiply_add_fusion
  10.4 1.2 convolution_convert_fusion.1
  11.6 19.2 %all_to_all.20 = bf16[8,1,48,512]{3,2,1,0:T(8,128)(2,1)} all-to-all(bf16[8,1,48,512]{3,2,1,0:T(8,128)(2,1)S(1)} %bitcast.163), channel_id=1, replica_groups=mesh['ep'=8,'tp'=4] {'ep'}, dimensions={0} | all-to-all | bytes 786432 | tf_op jit(solution)/shard_map/all_to_all | solution.py:47
  30.8 0.0 all-gather.3.cloned.1.call-update
  30.8 0.0 all-gather.5.cloned.1.call-start
  30.9 0.2 fusion.57
  31.2 0.2 select_reduce_fusion.2
  31.4 1.2 fusion.23
  32.5 15.1 %all_to_all.21 = bf16[8,1,48,512]{3,2,1,0:T(8,128)(2,1)} all-to-all(bf16[8,1,48,512]{3,2,1,0:T(8,128)(2,1)S(1)} %bitcast.162), channel_id=1, replica_groups=mesh['ep'=8,'tp'=4] {'ep'}, dimensions={0} | all-to-all | bytes 786432 | tf_op jit(solution)/shard_map/all_to_all | solution.py:54
  47.6 0.0 all-gather.5.cloned.1.call-update
  47.6 0.0 reduce-scatter.2.cloned.1.call-start
  47.7 1.6 %all-gather.3.cloned.1.call-done = bf16[8,1,48,2048]{3,2,0,1:T(8,128)(2,1)} async-done(((bf16[8,1,48,512]{3,2,0,1:T(8,128)(2,1)}), bf16[8,1,48,2048]{3,2,0,1:T(8,128)(2,1)}) %all-gather.3.cloned.1.call-update) | async-done | bytes 1572880 | tf_op jit(solution)/shard_map/all_gather | solution.py:63
  49.3 4.0 %fusion.2 = f32[8,48,512]{2,1,0:T(8,128)} fusion(bf16[1,2048,512]{2,1,0:T(8,128)(2,1)} %param.11, bf16[8,1,48,2048]{3,2,0,1:T(8,128)(2,1)} %all-gather.3.cloned.1.call-done), kind=kOutput, calls=%fused_computation.6 | convolution fusion | flops 805306368 | bytes 4456448 | tf_op jit(solution)/shard_map/slcd,ldf->slcf/dot_general | solution.py:67
  53.4 1.9 %fusion.8 = f32[8,48,512]{2,1,0:T(8,128)} fusion(bf16[1,2048,512]{2,1,0:T(8,128)(2,1)S(1)} %copy-done, bf16[8,1,48,2048]{3,2,0,1:T(8,128)(2,1)S(1)} %copy-done.5), kind=kOutput, calls=%fused_computation.12 | convolution fusion | flops 805306368 | bytes 4456448 | tf_op jit(solution)/shard_map/slcd,ldf->slcf/dot_general | solution.py:66
  55.2 15.3 %all-gather.5.cloned.1.call-done = bf16[8,1,48,2048]{3,2,0,1:T(8,128)(2,1)} async-done(((bf16[8,1,48,512]{3,2,0,1:T(8,128)(2,1)}), bf16[8,1,48,2048]{3,2,0,1:T(8,128)(2,1)}) %all-gather.5.cloned.1.call-update) | async-done | bytes 1572880 | tf_op jit(solution)/shard_map/all_gather | solution.py:64
  70.5 4.7 %multiply_reduce_fusion = (f32[8,48]{1,0:T(8,128)S(1)}, bf16[8,1,48,512]{3,2,0,1:T(8,128)(2,1)}, bf16[8,48,512]{2,1,0:T(8,128)(2,1)S(1)}, bf16[8,1,48,512]{3,2,0,1:T(8,128)(2,1)S(1)}) fusion(f32[8,48,512]{2,1,0:T(8,128)} %fusion.8, f32[8,48,512]{2,1,0:T(8,128)} %fusion.2, bf16[1,512,2048]{2,1,0:T(8,128)(2,1)} %param.12, ...), kind=kOutput, calls=%fused_computation.40 | convolution fusion | flops 810614400 | bytes 6424064 | tf_op jit(solution)/shard_map/slcd,lfd->slcf/dot_general | solution.py:73
  75.3 1.0 fusion.6
  76.3 0.5 copy-done.1
  76.9 2.2 %fusion = bf16[2048,8,1,48]{0,3,1,2:T(8,128)(2,1)} fusion(f32[8,48,2048]{2,1,0:T(8,128)S(1)} %fusion.6, bf16[8,48,512]{2,1,0:T(8,128)(2,1)S(1)} %get-tuple-element.9, bf16[1,2048,512]{2,1,0:T(8,128)(2,1)S(1)} %copy-done.1), kind=kOutput, calls=%fused_computation.4 | convolution fusion | flops 806879232 | bytes 7208960 | tf_op jit(solution)/shard_map/ldf,slcf->dslc/dot_general | solution.py:88
  79.1 0.0 reduce-scatter.2.cloned.1.call-update
  79.1 5.9 %psum.14 = bf16[8,1,48]{2,0,1:T(8,128)(2,1)S(1)} all-reduce(f32[8,1,48]{2,0,1:T(8,128)S(1)} %bitcast.166), channel_id=1, replica_groups=mesh['ep'=8,'tp'=4] {'tp'}, use_global_device_ids=true, to_apply=%region_9.10 | all-reduce | flops 384 | bytes 2304 | tf_op jit(solution)/shard_map/psum | solution.py:94
  85.0 0.6 copy.63
  85.6 5.7 %all-to-all-start.3 = ((bf16[1,8,1,48]{3,2,0,1:T(2,128)(2,1)}), bf16[1,8,1,48]{3,2,0,1:T(2,128)(2,1)S(1)}, u32[]{:S(2)}, u32[]{:S(2)}) async-start(bf16[1,8,1,48]{3,2,0,1:T(2,128)(2,1)} %copy.63), calls=%async_computation.4 | async-start | bytes 8192 | tf_op jit(solution)/shard_map/all_to_all | solution.py:99
  91.3 4.8 %convolution_bitcast_fusion.1 = f32[1,2048,512]{2,1,0:T(8,128)} fusion(bf16[8,48,512]{2,1,0:T(8,128)(2,1)S(1)} %get-tuple-element.9, bf16[8,1,48,2048]{3,2,0,1:T(8,128)(2,1)} %all-gather.3.cloned.1.call-done), kind=kOutput, calls=%fused_computation.1 | convolution fusion | flops 805306368 | bytes 6160384 | tf_op jit(solution)/shard_map/slcd,slcf->ldf/dot_general | solution.py:81
  96.1 3.3 %convolution_bitcast_fusion.2 = f32[1,2048,512]{2,1,0:T(8,128)} fusion(bf16[8,1,48,2048]{3,2,0,1:T(8,128)(2,1)S(1)} %copy-done.6, bf16[8,1,48,512]{3,2,0,1:T(8,128)(2,1)S(1)} %get-tuple-element.10), kind=kOutput, calls=%fused_computation.2 | convolution fusion | flops 805306368 | bytes 6160384 | tf_op jit(solution)/shard_map/slcd,slcf->ldf/dot_general | solution.py:80
  99.5 3.3 %convolution_bitcast_fusion = f32[1,512,2048]{2,1,0:T(8,128)} fusion(bf16[8,1,48,2048]{3,2,0,1:T(8,128)(2,1)S(1)} %copy-done.7, bf16[8,1,48,512]{3,2,0,1:T(8,128)(2,1)S(1)} %copy-done.8), kind=kOutput, calls=%fused_computation | convolution fusion | flops 805306368 | bytes 6160384 | tf_op jit(solution)/shard_map/slcf,slcd->lfd/dot_general | solution.py:82
  102.8 0.0 all-to-all-done.3
  102.8 0.1 reshape.152
  102.9 0.2 select_reduce_fusion
  103.1 4.2 %reduce-scatter.2.cloned.1.call-done = bf16[512,8,1,48]{0,3,1,2:T(8,128)(2,1)} async-done(((bf16[2048,8,1,48]{0,3,1,2:T(8,128)(2,1)}), bf16[512,8,1,48]{0,3,1,2:T(8,128)(2,1)}) %reduce-scatter.2.cloned.1.call-update) | async-done | bytes 393232 | tf_op jit(solution)/shard_map/reduce_scatter | solution.py:86
  107.3 5.5 %all-to-all-start.2 = ((bf16[512,8,1,48]{0,3,2,1:T(8,128)(2,1)}), bf16[512,8,1,48]{0,3,2,1:T(8,128)(2,1)S(1)}, u32[]{:S(2)}, u32[]{:S(2)}) async-start(bf16[512,8,1,48]{0,3,2,1:T(8,128)(2,1)} %bitcast.164), calls=%async_computation.3 | async-start | bytes 786432 | tf_op jit(solution)/shard_map/all_to_all | solution.py:96
  112.8 0.2 fusion.40
  113.0 38.3 %psum.15 = f32[512,8]{0,1:T(8,128)} all-reduce(f32[512,8]{0,1:T(8,128)S(1)} %fusion.40), channel_id=1, replica_groups=mesh['ep'=8,'tp'=4] {'ep'}, use_global_device_ids=true, to_apply=%region_13.14 | all-reduce | flops 4096 | bytes 32768 | tf_op jit(solution)/shard_map/psum | solution.py:122
  151.2 0.3 fusion.45
  151.5 0.0 all-to-all-done.2
  151.6 0.9 fusion.24
  (24 shorter events, 0.2 us)
Async XLA Ops:
  7.2 46.2 %copy-start = (bf16[1,2048,512]{2,1,0:T(8,128)(2,1)S(1)}, bf16[1,2048,512]{2,1,0:T(8,128)(2,1)}, u32[]{:S(2)}) copy-start(bf16[1,2048,512]{2,1,0:T(8,128)(2,1)} %param.10) | copy-start | bytes 6291460
  7.2 24.0 %copy-start.4 = (s32[128,2]{0,1:T(2,128)S(1)}, s32[128,2]{0,1:T(2,128)}, u32[]{:S(2)}) copy-start(s32[128,2]{0,1:T(2,128)} %param.8) | copy-start | bytes 3076
  7.2 23.7 %copy-start.2 = (bf16[128,2048]{1,0:T(8,128)(2,1)S(1)}, bf16[128,2048]{1,0:T(8,128)(2,1)}, u32[]{:S(2)}) copy-start(bf16[128,2048]{1,0:T(8,128)(2,1)} %param.7) | copy-start | bytes 1572868
  7.2 23.7 %copy-start.3 = (bf16[2048,8]{0,1:T(8,128)(2,1)S(1)}, bf16[2048,8]{0,1:T(8,128)(2,1)}, u32[]{:S(2)}) copy-start(bf16[2048,8]{0,1:T(8,128)(2,1)} %param.9) | copy-start | bytes 98308
  7.2 42.1 %all-gather.3.cloned.1.call-start = ((), (), s32[]{:S(2)}) async-start(), calls=%async_computation.5 | async-start | bytes 1966080 | tf_op jit(solution)/shard_map/all_gather | solution.py:63
  30.8 39.7 %all-gather.5.cloned.1.call-start = ((), (), s32[]{:S(2)}) async-start(), calls=%async_computation.6 | async-start | bytes 1966080 | tf_op jit(solution)/shard_map/all_gather | solution.py:64
  47.6 59.6 %reduce-scatter.2.cloned.1.call-start = ((), (), s32[]{:S(2)}) async-start(), calls=%async_computation.7 | async-start | bytes 1966080 | tf_op jit(solution)/shard_map/reduce_scatter | solution.py:86
  49.3 4.0 %copy-start.5 = (bf16[8,1,48,2048]{3,2,0,1:T(8,128)(2,1)S(1)}, bf16[8,1,48,2048]{3,2,0,1:T(8,128)(2,1)}, u32[]{:S(2)}) copy-start(bf16[8,1,48,2048]{3,2,0,1:T(8,128)(2,1)} %all-gather.3.cloned.1.call-done) | copy-start | bytes 4718596
  75.3 1.6 %copy-start.1 = (bf16[1,2048,512]{2,1,0:T(8,128)(2,1)S(1)}, bf16[1,2048,512]{2,1,0:T(8,128)(2,1)}, u32[]{:S(2)}) copy-start(bf16[1,2048,512]{2,1,0:T(8,128)(2,1)} %param.11) | copy-start | bytes 6291460
  85.6 17.2 %all-to-all-start.3 = ((bf16[1,8,1,48]{3,2,0,1:T(2,128)(2,1)}), bf16[1,8,1,48]{3,2,0,1:T(2,128)(2,1)S(1)}, u32[]{:S(2)}, u32[]{:S(2)}) async-start(bf16[1,8,1,48]{3,2,0,1:T(2,128)(2,1)} %copy.63), calls=%async_computation.4 | async-start | bytes 8192 | tf_op jit(solution)/shard_map/all_to_all | solution.py:99
  91.3 4.9 %copy-start.6 = (bf16[8,1,48,2048]{3,2,0,1:T(8,128)(2,1)S(1)}, bf16[8,1,48,2048]{3,2,0,1:T(8,128)(2,1)}, u32[]{:S(2)}) copy-start(bf16[8,1,48,2048]{3,2,0,1:T(8,128)(2,1)} %all-gather.3.cloned.1.call-done) | copy-start | bytes 4718596
  96.1 3.3 %copy-start.7 = (bf16[8,1,48,2048]{3,2,0,1:T(8,128)(2,1)S(1)}, bf16[8,1,48,2048]{3,2,0,1:T(8,128)(2,1)}, u32[]{:S(2)}) copy-start(bf16[8,1,48,2048]{3,2,0,1:T(8,128)(2,1)} %all-gather.5.cloned.1.call-done) | copy-start | bytes 4718596
  96.1 3.3 %copy-start.8 = (bf16[8,1,48,512]{3,2,0,1:T(8,128)(2,1)S(1)}, bf16[8,1,48,512]{3,2,0,1:T(8,128)(2,1)}, u32[]{:S(2)}) copy-start(bf16[8,1,48,512]{3,2,0,1:T(8,128)(2,1)} %get-tuple-element.8) | copy-start | bytes 1179652
  107.3 44.3 %all-to-all-start.2 = ((bf16[512,8,1,48]{0,3,2,1:T(8,128)(2,1)}), bf16[512,8,1,48]{0,3,2,1:T(8,128)(2,1)S(1)}, u32[]{:S(2)}, u32[]{:S(2)}) async-start(bf16[512,8,1,48]{0,3,2,1:T(8,128)(2,1)} %bitcast.164), calls=%async_computation.3 | async-start | bytes 786432 | tf_op jit(solution)/shard_map/all_to_all | solution.py:96
Sparse Core Ops, SparseCore 0:
  30.9 18.3 all-gather.2
  50.9 19.6 all-gather.4
  79.2 27.9 reduce-scatter.1
where the time goes:
time: 159 us
  blocking collectives  78.5 us (49%)
  matrix products  29.4 us (18%)
  waiting for transfers between devices  21.2 us (13%)
  between operations  13.9 us (9%)
  starting transfers between devices  11.3 us (7%)
  local copies, waits for them, and re-layouts  2.9 us (2%)
  other arithmetic  1.9 us (1%)
    psum x1, blocking collectives, on_device(): grad_router = lax.psum(router_part, 'ep')  38.3 us
    all_to_all x1, blocking collectives, on_device(): lax.all_to_all(token_slots.reshape(buffer_shape + (feature_part,)), 'ep',...  19.2 us
    all_gather x1, waiting for transfers between devices, on_device(): lax.all_gather(sent_cot, 'tp', axis=3, tiled=True)  15.3 us
    all_to_all x1, blocking collectives, on_device(): lax.all_to_all(scaled.reshape(buffer_shape + (feature_part,)), 'ep', spli...  15.1 us
    psum x1, blocking collectives, on_device(): share_sum = lax.psum(share_part, 'tp')  5.89 us
    all_to_all x1, starting transfers between devices, on_device(): lax.all_to_all(share_sum[None].astype(jnp.bfloat16), 'ep', split_axis=1,...  5.67 us
    all_to_all x1, starting transfers between devices, on_device(): lax.all_to_all(input_part.astype(jnp.bfloat16), 'ep', split_axis=1, conca...  5.51 us
    dot_general x1, matrix products, on_device(): jnp.einsum('slcd,slcf->ldf', arrived, d_up, preferred_element_type=jnp.fl...  4.85 us
  transfers between devices with their start and end apart: 5, of which 3 were waited for; matrix products, arithmetic and copies ran while one was open for 13% of the time, Pallas kernels for 0%

commit v1 on v0

--- a/solution.py
+++ b/solution.py
@@ -119,7 +119,10 @@
     router_part = lax.dot_general(
         token_cols.astype(jnp.float32), d_logits, (((0,), (0,)), ((), ())), precision=highest
     )
-    grad_router = lax.psum(router_part, "ep")
+    size, grad_router = (lax.axis_size("ep"), router_part)
+    for far in [1 << k for k in range(size.bit_length() - 1)]:
+        pairs = [(i, i ^ far) for i in range(size)]
+        grad_router = grad_router + lax.ppermute(grad_router, "ep", pairs)
     return (grad_tokens, grad_router, grad_gate, grad_up, grad_down)
 
 

time: 159 us -> 134 us (0.84)
  blocking collectives: 78.5 us -> 40.2 us
  starting transfers between devices: 11.3 us -> 16.1 us
  waiting for transfers between devices: 21.2 us -> 25.4 us
  matrix products: 29.4 us -> 32 us
    psum x1 -> x0, blocking collectives: 38.3 us -> none  [on_device(): grad_router = lax.psum(router_part, 'ep')]
    ppermute x0 -> x3, starting transfers between devices: none -> 4.84 us  [on_device(): grad_router = grad_router + lax.ppermute(grad_router, 'ep', pairs)]
    ppermute x0 -> x3, waiting for transfers between devices: none -> 4.25 us  [on_device(): grad_router = grad_router + lax.ppermute(grad_router, 'ep', pairs)]
    reduce_scatter x1, waiting for transfers between devices: 4.19 us -> 2.46 us  [on_device(): lax.psum_scatter((row_term + jnp.einsum('ldf,slcf->dslc', w_up, d_up, pre...]
    all_to_all x1, waiting for transfers between devices: 0.01 us -> 1.69 us  [on_device(): lax.all_to_all(share_sum[None].astype(jnp.bfloat16), 'ep', split_axis=1,...]
  transfers between devices with their start and end apart: 5 -> 8, of which waited for: 3 -> 5; matrix products, arithmetic and copies ran while one was open for 13% -> 18% of each run, Pallas kernels for 0% -> 0%
where the time goes in v1:
time: 134 us; the launch traced here: 133 us
  blocking collectives  40.2 us (30%)
  matrix products  32 us (24%)
  waiting for transfers between devices  25.4 us (19%)
  starting transfers between devices  16.1 us (12%)
  between operations  13.9 us (10%)
  local copies, waits for them, and re-layouts  2.9 us (2%)
  other arithmetic  2.52 us (2%)
    all_to_all x1, blocking collectives, on_device(): lax.all_to_all(token_slots.reshape(buffer_shape + (feature_part,)), 'ep',...  19.2 us
    all_gather x1, waiting for transfers between devices, on_device(): lax.all_gather(sent_cot, 'tp', axis=3, tiled=True)  15.3 us
    all_to_all x1, blocking collectives, on_device(): lax.all_to_all(scaled.reshape(buffer_shape + (feature_part,)), 'ep', spli...  15.1 us
    psum x1, blocking collectives, on_device(): share_sum = lax.psum(share_part, 'tp')  5.89 us
    all_to_all x1, starting transfers between devices, on_device(): lax.all_to_all(share_sum[None].astype(jnp.bfloat16), 'ep', split_axis=1,...  5.67 us
    all_to_all x1, starting transfers between devices, on_device(): lax.all_to_all(input_part.astype(jnp.bfloat16), 'ep', split_axis=1, conca...  5.51 us
    ppermute x3, starting transfers between devices, on_device(): grad_router = grad_router + lax.ppermute(grad_router, 'ep', pairs)  4.84 us
    dot_general x1, matrix products, on_device(): jnp.einsum('slcd,slcf->ldf', arrived, d_up, preferred_element_type=jnp.fl...  4.73 us
  transfers between devices with their start and end apart: 8, of which 5 were waited for; matrix products, arithmetic and copies ran while one was open for 18% of the time, Pallas kernels for 0%

profile of v1, /device:TPU:0, one launch (start us, length us, event | category | flops | bytes accessed | tf_op | source)
XLA Modules:
  0.0 133.0 jit_solution(7362965377217353769)
XLA Ops:
  7.2 0.0 all-gather.3.cloned.1.call-start
  7.3 0.9 copy.55
  8.2 0.1 eq.49
  8.3 0.1 eq.45
  8.5 0.6 reduce-window.6
  9.1 0.2 slice_reduce_fusion
  9.3 0.1 fusion.44
  9.4 0.1 reshape.140
  9.6 0.1 copy.57
  9.6 0.7 multiply_add_fusion
  10.4 1.2 convolution_convert_fusion.1
  11.6 19.2 %all_to_all.20 = bf16[8,1,48,512]{3,2,1,0:T(8,128)(2,1)} all-to-all(bf16[8,1,48,512]{3,2,1,0:T(8,128)(2,1)S(1)} %bitcast.163), channel_id=1, replica_groups=mesh['ep'=8,'tp'=4] {'ep'}, dimensions={0} | all-to-all | bytes 786432 | tf_op jit(solution)/shard_map/all_to_all | solution.py:47
  30.8 0.0 all-gather.3.cloned.1.call-update
  30.8 0.0 all-gather.5.cloned.1.call-start
  30.9 0.2 fusion.57
  31.2 0.2 select_reduce_fusion.2
  31.4 1.2 fusion.23
  32.5 15.1 %all_to_all.21 = bf16[8,1,48,512]{3,2,1,0:T(8,128)(2,1)} all-to-all(bf16[8,1,48,512]{3,2,1,0:T(8,128)(2,1)S(1)} %bitcast.162), channel_id=1, replica_groups=mesh['ep'=8,'tp'=4] {'ep'}, dimensions={0} | all-to-all | bytes 786432 | tf_op jit(solution)/shard_map/all_to_all | solution.py:54
  47.6 0.0 all-gather.5.cloned.1.call-update
  47.6 0.0 reduce-scatter.2.cloned.1.call-start
  47.7 1.6 %all-gather.3.cloned.1.call-done = bf16[8,1,48,2048]{3,2,0,1:T(8,128)(2,1)} async-done(((bf16[8,1,48,512]{3,2,0,1:T(8,128)(2,1)}), bf16[8,1,48,2048]{3,2,0,1:T(8,128)(2,1)}) %all-gather.3.cloned.1.call-update) | async-done | bytes 1572880 | tf_op jit(solution)/shard_map/all_gather | solution.py:63
  49.3 4.0 %fusion.2 = f32[8,48,512]{2,1,0:T(8,128)} fusion(bf16[1,2048,512]{2,1,0:T(8,128)(2,1)} %param.11, bf16[8,1,48,2048]{3,2,0,1:T(8,128)(2,1)} %all-gather.3.cloned.1.call-done), kind=kOutput, calls=%fused_computation.6 | convolution fusion | flops 805306368 | bytes 4456448 | tf_op jit(solution)/shard_map/slcd,ldf->slcf/dot_general | solution.py:67
  53.4 1.9 %fusion.8 = f32[8,48,512]{2,1,0:T(8,128)} fusion(bf16[1,2048,512]{2,1,0:T(8,128)(2,1)S(1)} %copy-done, bf16[8,1,48,2048]{3,2,0,1:T(8,128)(2,1)S(1)} %copy-done.5), kind=kOutput, calls=%fused_computation.12 | convolution fusion | flops 805306368 | bytes 4456448 | tf_op jit(solution)/shard_map/slcd,ldf->slcf/dot_general | solution.py:66
  55.2 15.3 %all-gather.5.cloned.1.call-done = bf16[8,1,48,2048]{3,2,0,1:T(8,128)(2,1)} async-done(((bf16[8,1,48,512]{3,2,0,1:T(8,128)(2,1)}), bf16[8,1,48,2048]{3,2,0,1:T(8,128)(2,1)}) %all-gather.5.cloned.1.call-update) | async-done | bytes 1572880 | tf_op jit(solution)/shard_map/all_gather | solution.py:64
  70.6 4.7 %multiply_reduce_fusion = (f32[8,48]{1,0:T(8,128)S(1)}, bf16[8,1,48,512]{3,2,0,1:T(8,128)(2,1)}, bf16[8,48,512]{2,1,0:T(8,128)(2,1)S(1)}, bf16[8,1,48,512]{3,2,0,1:T(8,128)(2,1)S(1)}) fusion(f32[8,48,512]{2,1,0:T(8,128)} %fusion.8, f32[8,48,512]{2,1,0:T(8,128)} %fusion.2, bf16[1,512,2048]{2,1,0:T(8,128)(2,1)} %param.12, ...), kind=kOutput, calls=%fused_computation.40 | convolution fusion | flops 810614400 | bytes 6424064 | tf_op jit(solution)/shard_map/slcd,lfd->slcf/dot_general | solution.py:73
  75.3 1.0 fusion.6
  76.3 0.6 copy-done.1
  76.9 2.2 %fusion = bf16[2048,8,1,48]{0,3,1,2:T(8,128)(2,1)} fusion(f32[8,48,2048]{2,1,0:T(8,128)S(1)} %fusion.6, bf16[8,48,512]{2,1,0:T(8,128)(2,1)S(1)} %get-tuple-element.9, bf16[1,2048,512]{2,1,0:T(8,128)(2,1)S(1)} %copy-done.1), kind=kOutput, calls=%fused_computation.4 | convolution fusion | flops 806879232 | bytes 7208960 | tf_op jit(solution)/shard_map/ldf,slcf->dslc/dot_general | solution.py:88
  79.0 0.0 reduce-scatter.2.cloned.1.call-update
  79.1 5.9 %psum.7 = bf16[8,1,48]{2,0,1:T(8,128)(2,1)S(1)} all-reduce(f32[8,1,48]{2,0,1:T(8,128)S(1)} %bitcast.166), channel_id=1, replica_groups=mesh['ep'=8,'tp'=4] {'tp'}, use_global_device_ids=true, to_apply=%region_9.10 | all-reduce | flops 384 | bytes 2304 | tf_op jit(solution)/shard_map/psum | solution.py:94
  84.9 0.6 copy.63
  85.5 5.7 %all-to-all-start.3 = ((bf16[1,8,1,48]{3,2,0,1:T(2,128)(2,1)}), bf16[1,8,1,48]{3,2,0,1:T(2,128)(2,1)S(1)}, u32[]{:S(2)}, u32[]{:S(2)}) async-start(bf16[1,8,1,48]{3,2,0,1:T(2,128)(2,1)} %copy.63), calls=%async_computation.4 | async-start | bytes 8192 | tf_op jit(solution)/shard_map/all_to_all | solution.py:99
  91.2 4.7 %convolution_bitcast_fusion.1 = f32[1,2048,512]{2,1,0:T(8,128)} fusion(bf16[8,48,512]{2,1,0:T(8,128)(2,1)S(1)} %get-tuple-element.9, bf16[8,1,48,2048]{3,2,0,1:T(8,128)(2,1)} %all-gather.3.cloned.1.call-done), kind=kOutput, calls=%fused_computation.1 | convolution fusion | flops 805306368 | bytes 6160384 | tf_op jit(solution)/shard_map/slcd,slcf->ldf/dot_general | solution.py:81
  95.9 1.7 %all-to-all-done.3 = bf16[1,8,1,48]{3,2,0,1:T(2,128)(2,1)S(1)} async-done(((bf16[1,8,1,48]{3,2,0,1:T(2,128)(2,1)}), bf16[1,8,1,48]{3,2,0,1:T(2,128)(2,1)S(1)}, u32[]{:S(2)}, u32[]{:S(2)}) %all-to-all-start.3) | async-done | bytes 800 | tf_op jit(solution)/shard_map/all_to_all | solution.py:99
  97.6 0.1 reshape.152
  97.7 0.2 select_reduce_fusion
  97.9 0.2 fusion.40
  98.1 0.6 collective-permute-start
  98.7 4.7 %convolution_bitcast_fusion.2 = f32[1,2048,512]{2,1,0:T(8,128)} fusion(bf16[8,1,48,2048]{3,2,0,1:T(8,128)(2,1)} %all-gather.3.cloned.1.call-done, bf16[8,1,48,512]{3,2,0,1:T(8,128)(2,1)S(1)} %get-tuple-element.10), kind=kOutput, calls=%fused_computation.2 | convolution fusion | flops 805306368 | bytes 6160384 | tf_op jit(solution)/shard_map/slcd,slcf->ldf/dot_general | solution.py:80
  103.4 1.3 collective-permute-start.1
  104.7 2.5 %reduce-scatter.2.cloned.1.call-done = bf16[512,8,1,48]{0,3,1,2:T(8,128)(2,1)} async-done(((bf16[2048,8,1,48]{0,3,1,2:T(8,128)(2,1)}), bf16[512,8,1,48]{0,3,1,2:T(8,128)(2,1)}) %reduce-scatter.2.cloned.1.call-update) | async-done | bytes 393232 | tf_op jit(solution)/shard_map/reduce_scatter | solution.py:86
  107.2 5.5 %all-to-all-start.2 = ((bf16[512,8,1,48]{0,3,2,1:T(8,128)(2,1)}), bf16[512,8,1,48]{0,3,2,1:T(8,128)(2,1)S(1)}, u32[]{:S(2)}, u32[]{:S(2)}) async-start(bf16[512,8,1,48]{0,3,2,1:T(8,128)(2,1)} %bitcast.164), calls=%async_computation.3 | async-start | bytes 786432 | tf_op jit(solution)/shard_map/all_to_all | solution.py:96
  112.7 4.7 %convolution_bitcast_fusion = f32[1,512,2048]{2,1,0:T(8,128)} fusion(bf16[8,1,48,2048]{3,2,0,1:T(8,128)(2,1)} %all-gather.5.cloned.1.call-done, bf16[8,1,48,512]{3,2,0,1:T(8,128)(2,1)S(1)} %copy-done.6), kind=kOutput, calls=%fused_computation | convolution fusion | flops 805306368 | bytes 6160384 | tf_op jit(solution)/shard_map/slcf,slcd->lfd/dot_general | solution.py:82
  117.4 3.0 %collective-permute-start.2 = (f32[512,8]{0,1:T(8,128)S(1)}, f32[512,8]{0,1:T(8,128)S(1)}, u32[]{:S(2)}, u32[]{:S(2)}) collective-permute-start(f32[512,8]{0,1:T(8,128)S(1)} %add.59), channel_id=1, source_target_pairs={{0,16},{4,20},{8,24},{12,28},{16,0},{20,4},{24,8},{28,12},{1,17},{... | collective-permute-start | bytes 49160 | tf_op jit(solution)/shard_map/ppermute | solution.py:125
  120.4 0.3 fusion.45
  120.7 4.2 %collective-permute-done.2 = f32[512,8]{0,1:T(8,128)S(1)} collective-permute-done((f32[512,8]{0,1:T(8,128)S(1)}, f32[512,8]{0,1:T(8,128)S(1)}, u32[]{:S(2)}, u32[]{:S(2)}) %collective-permute-start.2) | collective-permute-done | bytes 16416 | tf_op jit(solution)/shard_map/ppermute | solution.py:125
  125.0 0.6 add.60
  125.6 0.9 fusion.24
  (28 shorter events, 0.2 us)
Async XLA Ops:
  7.2 46.2 %copy-start = (bf16[1,2048,512]{2,1,0:T(8,128)(2,1)S(1)}, bf16[1,2048,512]{2,1,0:T(8,128)(2,1)}, u32[]{:S(2)}) copy-start(bf16[1,2048,512]{2,1,0:T(8,128)(2,1)} %param.10) | copy-start | bytes 6291460
  7.2 24.0 %copy-start.4 = (s32[128,2]{0,1:T(2,128)S(1)}, s32[128,2]{0,1:T(2,128)}, u32[]{:S(2)}) copy-start(s32[128,2]{0,1:T(2,128)} %param.8) | copy-start | bytes 3076
  7.2 23.7 %copy-start.2 = (bf16[128,2048]{1,0:T(8,128)(2,1)S(1)}, bf16[128,2048]{1,0:T(8,128)(2,1)}, u32[]{:S(2)}) copy-start(bf16[128,2048]{1,0:T(8,128)(2,1)} %param.7) | copy-start | bytes 1572868
  7.2 23.7 %copy-start.3 = (bf16[2048,8]{0,1:T(8,128)(2,1)S(1)}, bf16[2048,8]{0,1:T(8,128)(2,1)}, u32[]{:S(2)}) copy-start(bf16[2048,8]{0,1:T(8,128)(2,1)} %param.9) | copy-start | bytes 98308
  7.2 42.1 %all-gather.3.cloned.1.call-start = ((), (), s32[]{:S(2)}) async-start(), calls=%async_computation.5 | async-start | bytes 1966080 | tf_op jit(solution)/shard_map/all_gather | solution.py:63
  30.8 39.7 %all-gather.5.cloned.1.call-start = ((), (), s32[]{:S(2)}) async-start(), calls=%async_computation.6 | async-start | bytes 1966080 | tf_op jit(solution)/shard_map/all_gather | solution.py:64
  47.6 59.5 %reduce-scatter.2.cloned.1.call-start = ((), (), s32[]{:S(2)}) async-start(), calls=%async_computation.7 | async-start | bytes 1966080 | tf_op jit(solution)/shard_map/reduce_scatter | solution.py:86
  49.3 4.0 %copy-start.5 = (bf16[8,1,48,2048]{3,2,0,1:T(8,128)(2,1)S(1)}, bf16[8,1,48,2048]{3,2,0,1:T(8,128)(2,1)}, u32[]{:S(2)}) copy-start(bf16[8,1,48,2048]{3,2,0,1:T(8,128)(2,1)} %all-gather.3.cloned.1.call-done) | copy-start | bytes 4718596
  75.3 1.6 %copy-start.1 = (bf16[1,2048,512]{2,1,0:T(8,128)(2,1)S(1)}, bf16[1,2048,512]{2,1,0:T(8,128)(2,1)}, u32[]{:S(2)}) copy-start(bf16[1,2048,512]{2,1,0:T(8,128)(2,1)} %param.11) | copy-start | bytes 6291460
  85.5 12.1 %all-to-all-start.3 = ((bf16[1,8,1,48]{3,2,0,1:T(2,128)(2,1)}), bf16[1,8,1,48]{3,2,0,1:T(2,128)(2,1)S(1)}, u32[]{:S(2)}, u32[]{:S(2)}) async-start(bf16[1,8,1,48]{3,2,0,1:T(2,128)(2,1)} %copy.63), calls=%async_computation.4 | async-start | bytes 8192 | tf_op jit(solution)/shard_map/all_to_all | solution.py:99
  98.1 14.6 %copy-start.6 = (bf16[8,1,48,512]{3,2,0,1:T(8,128)(2,1)S(1)}, bf16[8,1,48,512]{3,2,0,1:T(8,128)(2,1)}, u32[]{:S(2)}) copy-start(bf16[8,1,48,512]{3,2,0,1:T(8,128)(2,1)} %get-tuple-element.8) | copy-start | bytes 1179652
  98.1 5.3 %collective-permute-start = (f32[512,8]{0,1:T(8,128)S(1)}, f32[512,8]{0,1:T(8,128)S(1)}, u32[]{:S(2)}, u32[]{:S(2)}) collective-permute-start(f32[512,8]{0,1:T(8,128)S(1)} %fusion.40), channel_id=1, source_target_pairs={{0,4},{4,0},{8,12},{12,8},{16,20},{20,16},{24,28},{28,24},{1,5},{5... | collective-permute-start | bytes 49160 | tf_op jit(solution)/shard_map/ppermute | solution.py:125
  103.4 14.0 %collective-permute-start.1 = (f32[512,8]{0,1:T(8,128)S(1)}, f32[512,8]{0,1:T(8,128)S(1)}, u32[]{:S(2)}, u32[]{:S(2)}) collective-permute-start(f32[512,8]{0,1:T(8,128)S(1)} %add.58), channel_id=1, source_target_pairs={{0,8},{4,12},{8,0},{12,4},{16,24},{20,28},{24,16},{28,20},{1,9},{5... | collective-permute-start | bytes 49160 | tf_op jit(solution)/shard_map/ppermute | solution.py:125
  107.2 18.4 %all-to-all-start.2 = ((bf16[512,8,1,48]{0,3,2,1:T(8,128)(2,1)}), bf16[512,8,1,48]{0,3,2,1:T(8,128)(2,1)S(1)}, u32[]{:S(2)}, u32[]{:S(2)}) async-start(bf16[512,8,1,48]{0,3,2,1:T(8,128)(2,1)} %bitcast.164), calls=%async_computation.3 | async-start | bytes 786432 | tf_op jit(solution)/shard_map/all_to_all | solution.py:96
  117.4 7.5 %collective-permute-start.2 = (f32[512,8]{0,1:T(8,128)S(1)}, f32[512,8]{0,1:T(8,128)S(1)}, u32[]{:S(2)}, u32[]{:S(2)}) collective-permute-start(f32[512,8]{0,1:T(8,128)S(1)} %add.59), channel_id=1, source_target_pairs={{0,16},{4,20},{8,24},{12,28},{16,0},{20,4},{24,8},{28,12},{1,17},{... | collective-permute-start | bytes 49160 | tf_op jit(solution)/shard_map/ppermute | solution.py:125
Sparse Core Ops, SparseCore 0:
  31.0 18.3 all-gather.2
  50.9 19.6 all-gather.4
  79.2 27.9 reduce-scatter.1
